TPU v7x, 32 devices: a whole 2x2x4 slice. The times are simulated.
32 devices in a mesh: ep: 16 (over z, y, x), tp: 2 (over core).
Axes of the slice: x: 2, y: 2, z: 4, core: 2. Of those that a mesh axis runs over, the one named last changes fastest.
Arguments:
- residual: bfloat16 [256, 2048], P(('ep', 'tp')), may hold values from -6 to 6
- query_latent: bfloat16 [256, 8, 512], P(('ep', 'tp')), may hold values from -40 to 40
- query_rotary: bfloat16 [256, 8, 32], P(('ep', 'tp')), may hold values from -6 to 6
- latent_new: bfloat16 [256, 512], P(('ep', 'tp')), may hold values from -16 to 16
- rotary_new: bfloat16 [256, 32], P(('ep', 'tp')), may hold values from -6 to 6
- latent_cache: bfloat16 [256, 256, 512], P(('ep', 'tp')), may hold values from -16 to 16
- rotary_cache: bfloat16 [256, 256, 32], P(('ep', 'tp')), may hold values from -6 to 6
- lengths: int32 [256], P(('ep', 'tp')), may hold values from 32 to 256, as said below
- value_up: bfloat16 [512, 8, 64], replicated, may hold values from -1 to 1
- out_proj: bfloat16 [512, 2048], replicated, may hold values from -0.5 to 0.5
- attn_gain: bfloat16 [2048], replicated, may hold values from 0.099609375 to 1.8984375
- mix_gate: bfloat16 [2048], replicated, may hold values from -0.125 to 0.125
- dense_w_gate: bfloat16 [2048, 2048], P(None, 'ep'), may hold values from -0.125 to 0.125
- dense_w_up: bfloat16 [2048, 2048], P(None, 'ep'), may hold values from -0.125 to 0.125
- dense_w_down: bfloat16 [2048, 2048], P('ep'), may hold values from -0.5 to 0.5
- expert_ids: int32 [256, 6], P(('ep', 'tp')), may hold values from 0 to 15, all different within a row; in each aligned block of 16 rows (0 to 15, 16 to 31, ...) at most 12 rows name the same one
- expert_scores: float32 [256, 6], P(('ep', 'tp')), may hold values from 0.1 to 5
- expert_gate: bfloat16 [16, 2048, 512], P('ep', None, 'tp'), may hold values from -0.125 to 0.125
- expert_up: bfloat16 [16, 2048, 512], P('ep', None, 'tp'), may hold values from -0.125 to 0.125
- expert_down: bfloat16 [16, 512, 2048], P('ep', 'tp'), may hold values from -1 to 1
- out_gain: bfloat16 [2048], replicated, may hold values from 0.099609375 to 1.8984375
Outputs:
- layer_out: bfloat16 [256, 2048], P(('ep', 'tp'))
Inputs may be any that keep to these rules, and one draw needn't show every extreme that they name: `expert_ids`: within each aligned block of 16 rows (the sequences of one ep index) no expert is named by more than 12 rows, a bound that some block reaches; a row names 6 different experts. `lengths`: some sequence has exactly 256 cached positions.
All inputs are finite; a program needn't handle non-finite values.
Results may differ from a plain program's by a relative error of at most 0.018.
Values may be sent and summed in bfloat16 or wider, within the bound.
No kernel may reach another device: no remote copies, remote signals or barrier semaphores. Data moves between devices by JAX's collectives and lax.ppermute only.
A program may use at most 128 MiB of HBM per device.

v0:
```python
import jax
import jax.numpy as jnp
from jax import lax
from jax.sharding import PartitionSpec as P

NOPE = 64


ALPHA = 8.0**0.25
EPS = 1e-06
ROPE_BASE = 10000.0


def rotate(vector, position):
    half_dim = vector.shape[-1] // 2
    inv_freq = ROPE_BASE ** (-jnp.arange(half_dim, dtype=jnp.float32) / half_dim)
    angles = position.astype(jnp.float32)[..., None] * inv_freq
    cosine = jnp.cos(angles)
    sine_part = jnp.sin(angles)
    lower_half = vector[..., :half_dim]
    upper_half = vector[..., half_dim:]
    return jnp.concatenate(
        [
            lower_half * cosine - upper_half * sine_part,
            upper_half * cosine + lower_half * sine_part,
        ],
        axis=-1,
    )


def normalize(values, gain):
    center = jnp.mean(values, -1, keepdims=True)
    spread = jnp.mean(jnp.square(values - center), -1, keepdims=True)
    return (values - center) * lax.rsqrt(spread + EPS) * gain.astype(jnp.float32)


def on_device(
    residual,
    query_latent,
    query_rotary,
    latent_new,
    rotary_new,
    latent_cache,
    rotary_cache,
    lengths,
    value_up,
    out_proj,
    attn_gain,
    mix_gate,
    dense_w_gate,
    dense_w_up,
    dense_w_down,
    expert_ids,
    expert_scores,
    expert_gate,
    expert_up,
    expert_down,
    out_gain,
):
    seq_count, model_width = residual.shape
    cache_len = latent_cache.shape[1]
    topk_count = expert_ids.shape[1]
    score_scale = (NOPE + query_rotary.shape[-1]) ** (-0.5)
    query_turned = rotate(query_rotary.astype(jnp.float32), lengths[:, None]).astype(jnp.bfloat16)
    key_turned = rotate(rotary_new.astype(jnp.float32), lengths).astype(jnp.bfloat16)
    scores = (
        jnp.einsum("bhr,btr->bht", query_latent, latent_cache, preferred_element_type=jnp.float32)
        + jnp.einsum("bhe,bte->bht", query_turned, rotary_cache, preferred_element_type=jnp.float32)
    ) * score_scale
    own_score = (
        jnp.einsum("bhr,br->bh", query_latent, latent_new, preferred_element_type=jnp.float32)
        + jnp.einsum("bhe,be->bh", query_turned, key_turned, preferred_element_type=jnp.float32)
    ) * score_scale
    live = jnp.arange(cache_len)[None, :] < lengths[:, None]
    scores = jnp.where(live[:, None, :], scores, -jnp.inf)
    top_score = jnp.maximum(jnp.max(scores, -1), own_score)
    cache_probs = jnp.exp(scores - top_score[..., None])
    own_prob = jnp.exp(own_score - top_score)
    prob_total = jnp.sum(cache_probs, -1) + own_prob
    cache_weights = (cache_probs / prob_total[..., None]).astype(jnp.bfloat16)
    own_weight = (own_prob / prob_total).astype(jnp.bfloat16)
    latent_out = (
        jnp.einsum("bht,btr->bhr", cache_weights, latent_cache, preferred_element_type=jnp.float32)
        + own_weight.astype(jnp.float32)[..., None] * latent_new.astype(jnp.float32)[:, None, :]
    ).astype(jnp.bfloat16)
    heads_out = jnp.einsum("bhr,rhv->bhv", latent_out, value_up, preferred_element_type=jnp.float32)
    heads_out = heads_out.astype(jnp.bfloat16).reshape(seq_count, -1)
    attn = jnp.dot(heads_out, out_proj, preferred_element_type=jnp.float32).astype(jnp.bfloat16)
    mixed = normalize(
        ALPHA * residual.astype(jnp.float32) + attn.astype(jnp.float32), attn_gain
    ).astype(jnp.bfloat16)
    mix = jax.nn.sigmoid(jnp.dot(mixed, mix_gate, preferred_element_type=jnp.float32))
    piece = lax.all_gather(mixed, "ep", axis=0, tiled=True)
    gate_pre = jnp.dot(piece, dense_w_gate, preferred_element_type=jnp.float32)
    up_pre = jnp.dot(piece, dense_w_up, preferred_element_type=jnp.float32)
    hidden_all = (jax.nn.silu(gate_pre) * up_pre).astype(jnp.bfloat16)
    dense_sum = lax.psum_scatter(
        jnp.dot(hidden_all, dense_w_down, preferred_element_type=jnp.float32),
        "ep",
        scatter_dimension=0,
        tiled=True,
    )
    dense_out = dense_sum.astype(jnp.bfloat16)
    group_rows, group_codes = (
        lax.all_gather(mixed, "tp", axis=0, tiled=True),
        lax.all_gather(expert_ids.astype(jnp.bfloat16), "tp", axis=0, tiled=True),
    )
    route_ids = group_codes.astype(jnp.int32).reshape(-1)
    group_tokens = group_rows.shape[0]
    expert_count = lax.axis_size("ep") * expert_gate.shape[0]
    slot_cap = max(2, 2 * group_tokens * topk_count // expert_count)
    onehot = (route_ids[:, None] == jnp.arange(expert_count, dtype=jnp.int32)[None, :]).astype(
        jnp.int32
    )
    slot_index = jnp.sum((jnp.cumsum(onehot, 0) - 1) * onehot, 1)
    outgoing = jnp.zeros((expert_count, slot_cap, model_width), jnp.bfloat16)
    outgoing = outgoing.at[route_ids, slot_index].set(jnp.repeat(group_rows, topk_count, axis=0))
    arrived = lax.all_to_all(outgoing, "ep", split_axis=0, concat_axis=0, tiled=True)
    sources, count, features = arrived.shape
    flat_rows = arrived.reshape(sources * count, features)
    gate_pre = jnp.dot(flat_rows, expert_gate[0], preferred_element_type=jnp.float32)
    up_pre = jnp.dot(flat_rows, expert_up[0], preferred_element_type=jnp.float32)
    hidden_part = (jax.nn.silu(gate_pre) * up_pre).astype(jnp.bfloat16)
    partial_value = jnp.dot(
        hidden_part, expert_down[0], preferred_element_type=jnp.float32
    ).reshape(sources, count, features)
    summed = lax.psum(partial_value.astype(jnp.bfloat16), "tp")
    returned = lax.all_to_all(summed, "ep", split_axis=0, concat_axis=0, tiled=True)
    own_slots = returned[route_ids, slot_index].reshape(group_tokens, topk_count, model_width)
    picked = lax.dynamic_slice_in_dim(own_slots, lax.axis_index("tp") * seq_count, seq_count, 0)
    route_share = expert_scores / jnp.sum(expert_scores, 1, keepdims=True)
    routed = jnp.sum(picked.astype(jnp.float32) * route_share[:, :, None], 1)
    summed_total = (
        ALPHA * mixed.astype(jnp.float32) + routed + mix[:, None] * dense_out.astype(jnp.float32)
    )
    return normalize(summed_total, out_gain).astype(jnp.bfloat16)


def solution(mesh):
    return jax.shard_map(
        on_device,
        mesh=mesh,
        in_specs=(
            P(("ep", "tp"), None),
            P(("ep", "tp"), None, None),
            P(("ep", "tp"), None, None),
            P(("ep", "tp"), None),
            P(("ep", "tp"), None),
            P(("ep", "tp"), None, None),
            P(("ep", "tp"), None, None),
            P(("ep", "tp")),
            P(),
            P(),
            P(),
            P(),
            P(None, "ep"),
            P(None, "ep"),
            P("ep", None),
            P(("ep", "tp"), None),
            P(("ep", "tp"), None),
            P("ep", None, "tp"),
            P("ep", None, "tp"),
            P("ep", "tp", None),
            P(),
        ),
        out_specs=P(("ep", "tp"), None),
        check_vma=False,
    )
```

profile of v0, /device:TPU:0, one launch (start us, length us, event | category | flops | bytes accessed | tf_op | source)
XLA Modules:
  0.0 203.7 jit_solution(17127304516886828509)
XLA Ops:
  7.4 0.9 iota_compare_fusion.1
  9.7 2.0 all_gather.9
  12.5 0.7 convert_element_type.86
  13.2 0.7 convert_element_type.92
  13.9 1.5 fusion.45
  17.4 2.1 %fusion.44 = (f32[8]{0:T(128)S(1)}, f32[8,2048]{1,0:T(8,128)S(1)}) fusion(bf16[8,512]{1,0:T(8,128)(2,1)S(1)} %reshape.178, bf16[512,2048]{1,0:T(8,128)(2,1)} %param.30, bf16[8,2048]{1,0:T(8,128)(2,1)S(1)} %copy-done.6), kind=kOutput, calls=%fused_computation.86 | convolution fusion | flops 16875512 | bytes 2203680 | tf_op jit(solution)/shard_map/dot_general | solution.py:88
  19.8 1.9 all_gather.10
  22.4 9.0 %scatter_fusion = bf16[16,12,2048]{2,0,1:T(8,128)(2,1)S(1)} fusion(bf16[16,12,2048]{2,0,1:T(8,128)(2,1)S(1)} %broadcast_in_dim.18, s32[96]{0:T(128)S(1)} %get-tuple-element.7, bf16[96,2048]{1,0:T(8,128)(2,1)S(1)} %reshape.191), kind=kCustom, calls=%fused_computation.1 | custom fusion | bytes 1180416 | tf_op jit(solution)/shard_map/scatter | solution.py:117
  31.9 34.6 %all_to_all.10 = bf16[16,12,2048]{2,1,0:T(8,128)(2,1)S(1)} all-to-all(bf16[16,12,2048]{2,1,0:T(8,128)(2,1)S(1)} %copy.30), channel_id=1, replica_groups=mesh['ep'=16,'tp'=2] {'ep'}, dimensions={0} | all-to-all | bytes 1572864 | tf_op jit(solution)/shard_map/all_to_all | solution.py:118
  66.5 1.1 reshape.181
  67.6 1.9 fusion.15
  69.5 1.8 fusion.2
  71.4 1.3 convolution_convert_fusion
  72.8 41.5 %all_gather.11 = bf16[128,2048]{1,0:T(8,128)(2,1)S(1)} all-gather(bf16[8,2048]{1,0:T(8,128)(2,1)S(1)} %multiply_convert_fusion.1), channel_id=1, replica_groups=mesh['ep'=16,'tp'=2] {'ep'}, dimensions={0}, use_global_device_ids=true | all-gather | bytes 557056 | tf_op jit(solution)/shard_map/all_gather | solution.py:93
  114.3 1.3 fusion.46
  115.6 2.6 %fusion.7 = f32[128,2048]{1,0:T(8,128)} fusion(bf16[128,2048]{1,0:T(8,128)(2,1)S(1)} %copy-done.3, bf16[128,2048]{1,0:T(8,128)(2,1)S(1)} %all_gather.11, bf16[2048,128]{1,0:T(8,128)(2,1)} %param.34, f32[128,128]{1,0:T(8,128)S(1)} %fusion.46), kind=kOutput, calls=%fused_computation.15 | convolution fusion | flops 134316032 | bytes 2686976 | tf_op jit(solution)/shard_map/dot_general | solution.py:98
  118.3 2.6 %copy.32 = bf16[16,12,2048]{2,1,0:T(8,128)(2,1)} copy(bf16[16,12,2048]{2,0,1:T(8,128)(2,1)} %all-reduce.2.cloned.1.call-done) | data formatting | bytes 1572864 | tf_op jit(solution)/shard_map/psum | solution.py:127
  120.9 4.3 %all-to-all-start.1 = ((bf16[16,12,2048]{2,1,0:T(8,128)(2,1)}), bf16[16,12,2048]{2,1,0:T(8,128)(2,1)}, u32[]{:S(2)}, u32[]{:S(2)}) async-start(bf16[16,12,2048]{2,1,0:T(8,128)(2,1)} %copy.32), calls=%async_computation.1 | async-start | bytes 2097152 | tf_op jit(solution)/shard_map/all_to_all | solution.py:128
  125.7 21.3 %all-to-all-done.1 = bf16[16,12,2048]{2,1,0:T(8,128)(2,1)} async-done(((bf16[16,12,2048]{2,1,0:T(8,128)(2,1)}), bf16[16,12,2048]{2,1,0:T(8,128)(2,1)}, u32[]{:S(2)}, u32[]{:S(2)}) %all-to-all-start.1) | async-done | bytes 786464 | tf_op jit(solution)/shard_map/all_to_all | solution.py:128
  147.0 1.7 copy.33
  148.6 2.5 %gather_fusion = bf16[96,2048]{1,0:T(8,128)(2,1)S(1)} fusion(bf16[16,12,2048]{2,0,1:T(8,128)(2,1)S(1)} %copy.33, s32[96]{0:T(128)S(1)} %bitcast.56), kind=kCustom, calls=%fused_computation | custom fusion | bytes 787200 | tf_op jit(solution)/shard_map/gather | solution.py:129
  151.6 42.7 %reduce-scatter.2.cloned.1.call-done = f32[8,2048]{1,0:T(8,128)} async-done(((f32[128,2048]{1,0:T(8,128)}), f32[8,2048]{1,0:T(8,128)}) %reduce-scatter.2.cloned.1.call-update) | async-done | bytes 65552 | tf_op jit(solution)/shard_map/reduce_scatter | solution.py:97
  194.3 1.0 fusion.41
  195.6 0.7 multiply_convert_fusion
  (73 shorter events, 6.6 us)
Async XLA Ops:
  7.4 6.6 %copy-start = (bf16[8,256,512]{2,1,0:T(8,128)(2,1)S(1)}, bf16[8,256,512]{2,1,0:T(8,128)(2,1)}, u32[]{:S(2)}) copy-start(bf16[8,256,512]{2,1,0:T(8,128)(2,1)} %param.26) | copy-start | bytes 6291460
  7.4 8.1 %copy-start.8 = (bf16[8,512]{1,0:T(8,128)(2,1)S(1)}, bf16[8,512]{1,0:T(8,128)(2,1)}, u32[]{:S(2)}) copy-start(bf16[8,512]{1,0:T(8,128)(2,1)} %param.24) | copy-start | bytes 24580
  7.4 8.1 %copy-start.5 = (bf16[8,8,512]{2,1,0:T(8,128)(2,1)S(1)}, bf16[8,8,512]{2,1,0:T(8,128)(2,1)}, u32[]{:S(2)}) copy-start(bf16[8,8,512]{2,1,0:T(8,128)(2,1)} %param.22) | copy-start | bytes 196612
  7.4 8.7 %copy-start.4 = (bf16[8,256,32]{1,2,0:T(8,128)(2,1)S(1)}, bf16[8,256,32]{1,2,0:T(8,128)(2,1)}, u32[]{:S(2)}) copy-start(bf16[8,256,32]{1,2,0:T(8,128)(2,1)} %param.27) | copy-start | bytes 393220
  7.4 110.9 %all-reduce.2.cloned.1.call-start = ((), (), s32[]{:S(2)}) async-start(), calls=%async_computation.3 | async-start | bytes 1572864 | tf_op jit(solution)/shard_map/psum | solution.py:127
  13.9 3.1 %copy-start.2 = (bf16[512,8,64]{0,2,1:T(8,128)(2,1)S(1)}, bf16[512,8,64]{0,2,1:T(8,128)(2,1)}, u32[]{:S(2)}) copy-start(bf16[512,8,64]{0,2,1:T(8,128)(2,1)} %param.29) | copy-start | bytes 1572868
  15.5 1.9 copy-start.6
  16.6 3.1 %copy-start.9 = (bf16[2048]{0:T(1024)(128)(2,1)S(1)}, bf16[2048]{0:T(1024)(128)(2,1)}, u32[]{:S(2)}) copy-start(bf16[2048]{0:T(1024)(128)(2,1)} %param.31) | copy-start | bytes 12292
  67.6 3.8 %copy-start.1 = (bf16[1,256,2048]{2,1,0:T(8,128)(2,1)S(1)}, bf16[1,256,2048]{2,1,0:T(8,128)(2,1)}, u32[]{:S(2)}) copy-start(bf16[1,256,2048]{2,1,0:T(8,128)(2,1)} %param.40) | copy-start | bytes 3145732
  72.7 42.9 %copy-start.3 = (bf16[128,2048]{1,0:T(8,128)(2,1)S(1)}, bf16[128,2048]{1,0:T(8,128)(2,1)}, u32[]{:S(2)}) copy-start(bf16[128,2048]{1,0:T(8,128)(2,1)} %param.35) | copy-start | bytes 1572868
  72.7 121.6 %reduce-scatter.2.cloned.1.call-start = ((), (), s32[]{:S(2)}) async-start(), calls=%async_computation.4 | async-start | bytes 1114112 | tf_op jit(solution)/shard_map/reduce_scatter | solution.py:97
  118.2 7.0 %copy-start.10 = (bf16[2048]{0:T(1024)(128)(2,1)S(1)}, bf16[2048]{0:T(1024)(128)(2,1)}, u32[]{:S(2)}) copy-start(bf16[2048]{0:T(1024)(128)(2,1)} %param.32) | copy-start | bytes 12292
  118.2 7.1 %copy-start.11 = (bf16[2048]{0:T(1024)(128)(2,1)S(1)}, bf16[2048]{0:T(1024)(128)(2,1)}, u32[]{:S(2)}) copy-start(bf16[2048]{0:T(1024)(128)(2,1)} %param.41) | copy-start | bytes 12292
  118.3 7.1 %copy-start.7 = (f32[8,6]{1,0:T(8,128)S(1)}, f32[8,6]{1,0:T(8,128)}, u32[]{:S(2)}) copy-start(f32[8,6]{1,0:T(8,128)} %param.37) | copy-start | bytes 580
  120.9 26.0 %all-to-all-start.1 = ((bf16[16,12,2048]{2,1,0:T(8,128)(2,1)}), bf16[16,12,2048]{2,1,0:T(8,128)(2,1)}, u32[]{:S(2)}, u32[]{:S(2)}) async-start(bf16[16,12,2048]{2,1,0:T(8,128)(2,1)} %copy.32), calls=%async_computation.1 | async-start | bytes 2097152 | tf_op jit(solution)/shard_map/all_to_all | solution.py:128
Sparse Core Ops, SparseCore 0:
  72.8 17.2 all-reduce.1
Sparse Core Ops, SparseCore 1:
  118.3 75.9 reduce-scatter.1
where the time goes:
time: 204 us
  blocking collectives  80 us (39%)
  waiting for transfers between devices  64.1 us (31%)
  local copies, waits for them, and re-layouts  18.1 us (9%)
  between operations  15.1 us (7%)
  matrix products  14 us (7%)
  other arithmetic  7.9 us (4%)
  starting transfers between devices  4.41 us (2%)
    reduce_scatter x1, waiting for transfers between devices, on_device(): lax.psum_scatter(jnp.dot(hidden_all, dense_w_down, preferred_element_type...  42.7 us
    all_gather x1, blocking collectives, on_device(): piece = lax.all_gather(mixed, 'ep', axis=0, tiled=True)  41.5 us
    all_to_all x1, blocking collectives, on_device(): lax.all_to_all(outgoing, 'ep', split_axis=0, concat_axis=0, tiled=True)  34.6 us
    all_to_all x1, waiting for transfers between devices, on_device(): lax.all_to_all(summed, 'ep', split_axis=0, concat_axis=0, tiled=True)  21.3 us
    scatter x2, local copies, waits for them, and re-layouts, on_device(): outgoing.at[route_ids, slot_index]  9.47 us
    all_to_all x1, starting transfers between devices, on_device(): lax.all_to_all(summed, 'ep', split_axis=0, concat_axis=0, tiled=True)  4.34 us
  transfers between devices with their start and end apart: 3, of which 2 were waited for; matrix products, arithmetic and copies ran while one was open for 6% of the time, Pallas kernels for 0%

commit v1 on v0

--- a/solution.py
+++ b/solution.py
@@ -4,6 +4,7 @@
 from jax.sharding import PartitionSpec as P
 
 NOPE = 64
+LANES = 128
 
 
 ALPHA = 8.0**0.25
@@ -34,6 +35,13 @@
     return (values - center) * lax.rsqrt(spread + EPS) * gain.astype(jnp.float32)
 
 
+def gated(rows, gate_weight, up_weight, down_weight):
+    gate_pre = jnp.dot(rows, gate_weight, preferred_element_type=jnp.float32)
+    up_pre = jnp.dot(rows, up_weight, preferred_element_type=jnp.float32)
+    hidden = (jax.nn.silu(gate_pre) * up_pre).astype(jnp.bfloat16)
+    return jnp.dot(hidden, down_weight, preferred_element_type=jnp.float32)
+
+
 def on_device(
     residual,
     query_latent,
@@ -59,7 +67,11 @@
 ):
     seq_count, model_width = residual.shape
     cache_len = latent_cache.shape[1]
-    topk_count = expert_ids.shape[1]
+    tp_count = lax.axis_size("tp")
+    swap = [(i, (i + 1) % tp_count) for i in range(tp_count)]
+    other_gate = lax.ppermute(expert_gate, "tp", swap)
+    other_up = lax.ppermute(expert_up, "tp", swap)
+    other_down = lax.ppermute(expert_down, "tp", swap)
     score_scale = (NOPE + query_rotary.shape[-1]) ** (-0.5)
     query_turned = rotate(query_rotary.astype(jnp.float32), lengths[:, None]).astype(jnp.bfloat16)
     key_turned = rotate(rotary_new.astype(jnp.float32), lengths).astype(jnp.bfloat16)
@@ -89,50 +101,36 @@
     mixed = normalize(
         ALPHA * residual.astype(jnp.float32) + attn.astype(jnp.float32), attn_gain
     ).astype(jnp.bfloat16)
-    mix = jax.nn.sigmoid(jnp.dot(mixed, mix_gate, preferred_element_type=jnp.float32))
-    piece = lax.all_gather(mixed, "ep", axis=0, tiled=True)
-    gate_pre = jnp.dot(piece, dense_w_gate, preferred_element_type=jnp.float32)
-    up_pre = jnp.dot(piece, dense_w_up, preferred_element_type=jnp.float32)
-    hidden_all = (jax.nn.silu(gate_pre) * up_pre).astype(jnp.bfloat16)
-    dense_sum = lax.psum_scatter(
-        jnp.dot(hidden_all, dense_w_down, preferred_element_type=jnp.float32),
+    ep_count = lax.axis_size("ep")
+    route_share = expert_scores / jnp.sum(expert_scores, 1, keepdims=True)
+    chosen = expert_ids[None] == jnp.arange(ep_count, dtype=jnp.int32)[:, None, None]
+    weight_of = jnp.sum(jnp.where(chosen, route_share[None], 0.0), -1)
+    coarse = lax.reduce_precision(weight_of, 8, 7)
+    lane = lax.broadcasted_iota(jnp.int32, (ep_count, seq_count, LANES), 2)
+    tail = jnp.where(
+        lane == 0, coarse[..., None], jnp.where(lane == 1, (weight_of - coarse)[..., None], 0.0)
+    ).astype(jnp.bfloat16)
+    outgoing = jnp.concatenate(
+        [jnp.broadcast_to(mixed[None], (ep_count, seq_count, model_width)), tail], -1
+    )
+    arrived = lax.all_to_all(outgoing, "ep", split_axis=0, concat_axis=0, tiled=True)
+    arrived = arrived.reshape(ep_count * seq_count, model_width + LANES)
+    rows = arrived[:, :model_width]
+    weight = jnp.sum(arrived[:, model_width:].astype(jnp.float32), -1, keepdims=True)
+    partial_value = gated(rows, expert_gate[0], expert_up[0], expert_down[0]) + gated(
+        rows, other_gate[0], other_up[0], other_down[0]
+    )
+    mix = jax.nn.sigmoid(jnp.dot(rows, mix_gate, preferred_element_type=jnp.float32))
+    dense_part = gated(rows, dense_w_gate, dense_w_up, dense_w_down)
+    combined = (weight * partial_value + mix[:, None] * dense_part).astype(jnp.bfloat16)
+    returned = lax.all_to_all(
+        combined.reshape(ep_count, seq_count, model_width),
         "ep",
-        scatter_dimension=0,
+        split_axis=0,
+        concat_axis=0,
         tiled=True,
     )
-    dense_out = dense_sum.astype(jnp.bfloat16)
-    group_rows, group_codes = (
-        lax.all_gather(mixed, "tp", axis=0, tiled=True),
-        lax.all_gather(expert_ids.astype(jnp.bfloat16), "tp", axis=0, tiled=True),
-    )
-    route_ids = group_codes.astype(jnp.int32).reshape(-1)
-    group_tokens = group_rows.shape[0]
-    expert_count = lax.axis_size("ep") * expert_gate.shape[0]
-    slot_cap = max(2, 2 * group_tokens * topk_count // expert_count)
-    onehot = (route_ids[:, None] == jnp.arange(expert_count, dtype=jnp.int32)[None, :]).astype(
-        jnp.int32
-    )
-    slot_index = jnp.sum((jnp.cumsum(onehot, 0) - 1) * onehot, 1)
-    outgoing = jnp.zeros((expert_count, slot_cap, model_width), jnp.bfloat16)
-    outgoing = outgoing.at[route_ids, slot_index].set(jnp.repeat(group_rows, topk_count, axis=0))
-    arrived = lax.all_to_all(outgoing, "ep", split_axis=0, concat_axis=0, tiled=True)
-    sources, count, features = arrived.shape
-    flat_rows = arrived.reshape(sources * count, features)
-    gate_pre = jnp.dot(flat_rows, expert_gate[0], preferred_element_type=jnp.float32)
-    up_pre = jnp.dot(flat_rows, expert_up[0], preferred_element_type=jnp.float32)
-    hidden_part = (jax.nn.silu(gate_pre) * up_pre).astype(jnp.bfloat16)
-    partial_value = jnp.dot(
-        hidden_part, expert_down[0], preferred_element_type=jnp.float32
-    ).reshape(sources, count, features)
-    summed = lax.psum(partial_value.astype(jnp.bfloat16), "tp")
-    returned = lax.all_to_all(summed, "ep", split_axis=0, concat_axis=0, tiled=True)
-    own_slots = returned[route_ids, slot_index].reshape(group_tokens, topk_count, model_width)
-    picked = lax.dynamic_slice_in_dim(own_slots, lax.axis_index("tp") * seq_count, seq_count, 0)
-    route_share = expert_scores / jnp.sum(expert_scores, 1, keepdims=True)
-    routed = jnp.sum(picked.astype(jnp.float32) * route_share[:, :, None], 1)
-    summed_total = (
-        ALPHA * mixed.astype(jnp.float32) + routed + mix[:, None] * dense_out.astype(jnp.float32)
-    )
+    summed_total = ALPHA * mixed.astype(jnp.float32) + jnp.sum(returned.astype(jnp.float32), 0)
     return normalize(summed_total, out_gain).astype(jnp.bfloat16)
 
 

time: 204 us -> 69.1 us (0.34)
  blocking collectives: 80 us -> 0 us
  waiting for transfers between devices: 64.1 us -> 29.4 us
  local copies, waits for them, and re-layouts: 18.1 us -> 0.57 us
  between operations: 15.1 us -> 0.27 us
  starting transfers between devices: 4.41 us -> 13.1 us
  matrix products: 14 us -> 18.2 us
    all_gather x3 -> x0, blocking collectives: 45.4 us -> none  [the longest x1 41.5 us: on_device(): piece = lax.all_gather(mixed, 'ep', axis=0, tiled=True)]
    reduce_scatter x1 -> x0, waiting for transfers between devices: 42.7 us -> none  [on_device(): lax.psum_scatter(jnp.dot(hidden_all, dense_w_down, preferred_element_type...]
    all_to_all x1 -> x0, blocking collectives: 34.6 us -> none  [on_device(): lax.all_to_all(outgoing, 'ep', split_axis=0, concat_axis=0, tiled=True)]
    scatter x2 -> x0, local copies, waits for them, and re-layouts: 9.47 us -> none  [on_device(): outgoing.at[route_ids, slot_index]]
    all_to_all x1 -> x2, starting transfers between devices: 4.34 us -> 12.4 us  [the longest x1 8.35 us: on_device(): lax.all_to_all(outgoing, 'ep', split_axis=0, concat_axis=0, tiled=True)]
    all_to_all x1 -> x2, waiting for transfers between devices: 21.3 us -> 29.4 us  [the longest x1 15 us: on_device(): lax.all_to_all(outgoing, 'ep', split_axis=0, concat_axis=0, tiled=True)]
    dot_general x6 -> x7, matrix products: 9.11 us -> 13.3 us  [the longest x3 9.72 us: gated(): return jnp.dot(hidden, down_weight, preferred_element_type=jnp.float32)]
    psum x1 -> x0, local copies, waits for them, and re-layouts: 2.62 us -> none  [on_device(): summed = lax.psum(partial_value.astype(jnp.bfloat16), 'tp')]
  transfers between devices with their start and end apart: 3 -> 5, of which waited for: 2 -> 2; matrix products, arithmetic and copies ran while one was open for 6% -> 10% of each run, Pallas kernels for 0% -> 0%
where the time goes in v1:
time: 69.1 us; the launch traced here: 68.5 us
  waiting for transfers between devices  29.4 us (43%)
  matrix products  18.2 us (26%)
  starting transfers between devices  13.1 us (19%)
  other arithmetic  6.96 us (10%)
    all_to_all x1, waiting for transfers between devices, on_device(): lax.all_to_all(outgoing, 'ep', split_axis=0, concat_axis=0, tiled=True)  15 us
    all_to_all x1, waiting for transfers between devices, on_device(): lax.all_to_all(combined.reshape(ep_count, seq_count, model_width), 'ep',...  14.4 us
    dot_general x3, matrix products, gated(): return jnp.dot(hidden, down_weight, preferred_element_type=jnp.float32)  9.72 us
    all_to_all x1, starting transfers between devices, on_device(): lax.all_to_all(outgoing, 'ep', split_axis=0, concat_axis=0, tiled=True)  8.35 us
    all_to_all x1, starting transfers between devices, on_device(): lax.all_to_all(combined.reshape(ep_count, seq_count, model_width), 'ep',...  4.08 us
    dot_general x1, matrix products, on_device(): jnp.dot(heads_out, out_proj, preferred_element_type=jnp.float32)  2.1 us
    dot_general x2, matrix products, gated(): gate_pre = jnp.dot(rows, gate_weight, preferred_element_type=jnp.float32)  1.85 us
    dot_general x1, matrix products, on_device(): jnp.einsum('bhr,btr->bht', query_latent, latent_cache, preferred_element_...  1.53 us
  transfers between devices with their start and end apart: 5, of which 2 were waited for; matrix products, arithmetic and copies ran while one was open for 10% of the time, Pallas kernels for 0%

profile of v1, /device:TPU:0, one launch (start us, length us, event | category | flops | bytes accessed | tf_op | source)
XLA Modules:
  0.0 68.5 jit_solution(8129326523280967378)
XLA Ops:
  0.0 0.8 %convert_element_type.81 = f32[8]{0:T(128)S(1)} convert(s32[8]{0:T(128)} %param.28) | non-fusion elementwise | flops 8 | bytes 64 | tf_op jit(solution)/shard_map/convert_element_type | solution.py:18
  0.8 0.7 %iota_compare_fusion.1 = pred[8,256]{1,0:T(8,128)(4,1)S(1)} fusion(s32[8]{0:T(128)} %param.28), kind=kLoop, calls=%fused_computation.80 | loop fusion | flops 2048 | bytes 2080 | tf_op jit(solution)/shard_map/lt | solution.py:86
  1.6 0.7 convert_element_type.82
  2.3 0.7 %convert_element_type.80 = f32[8,8,32]{2,1,0:T(8,128)S(1)} convert(bf16[8,8,32]{2,1,0:T(8,128)(2,1)} %param.23) | non-fusion elementwise | flops 2048 | bytes 12288 | tf_op jit(solution)/shard_map/convert_element_type | solution.py:76
  3.0 0.7 %convert_element_type.86 = f32[8,512]{1,0:T(8,128)S(1)} convert(bf16[8,512]{1,0:T(8,128)(2,1)} %param.24) | non-fusion elementwise | flops 4096 | bytes 24576 | tf_op jit(solution)/shard_map/convert_element_type | solution.py:96
  3.7 1.5 %fusion.78 = f32[8,8,256]{2,1,0:T(8,128)S(1)} fusion(bf16[8,8,512]{2,1,0:T(8,128)(2,1)} %param.22, bf16[8,256,512]{2,1,0:T(8,128)(2,1)S(1)} %copy-done), kind=kOutput, calls=%fused_computation.111 | convolution fusion | flops 16777216 | bytes 2228224 | tf_op jit(solution)/shard_map/bhr,btr->bht/dot_general | solution.py:79
  5.9 0.3 fusion.76
  6.4 0.4 fusion.7
  6.8 0.2 fusion.12
  7.2 2.1 %fusion.77 = (f32[8]{0:T(128)S(1)}, f32[8,2048]{1,0:T(8,128)S(1)}) fusion(bf16[8,512]{1,0:T(8,128)(2,1)S(1)} %reshape.137, bf16[512,2048]{1,0:T(8,128)(2,1)} %param.30, bf16[8,2048]{1,0:T(8,128)(2,1)S(1)} %copy-done.6), kind=kOutput, calls=%fused_computation.110 | convolution fusion | flops 16875512 | bytes 2203680 | tf_op jit(solution)/shard_map/dot_general | solution.py:100
  10.4 0.8 %pad_maximum_fusion = bf16[16,8,2176]{2,1,0:T(8,128)(2,1)} fusion(bf16[16,8,128]{2,1,0:T(8,128)(2,1)S(1)} %select_convert_fusion, bf16[16,8,2048]{2,1,0:T(8,128)(2,1)S(1)} %broadcast_in_dim.45), kind=kLoop, calls=%fused_computation.36 | loop fusion | flops 1114112 | bytes 1114112 | tf_op jit(solution)/shard_map/concatenate | solution.py:113
  11.3 8.4 %all-to-all-start = ((bf16[16,8,2176]{2,1,0:T(8,128)(2,1)}), bf16[16,8,2176]{2,1,0:T(8,128)(2,1)S(1)}, u32[]{:S(2)}, u32[]{:S(2)}) async-start(bf16[16,8,2176]{2,1,0:T(8,128)(2,1)} %pad_maximum_fusion), calls=%async_computation | async-start | bytes 1114112 | tf_op jit(solution)/shard_map/all_to_all | solution.py:116
  19.7 0.5 collective-permute-start
  20.3 15.0 %all-to-all-done = bf16[16,8,2176]{2,1,0:T(8,128)(2,1)S(1)} async-done(((bf16[16,8,2176]{2,1,0:T(8,128)(2,1)}), bf16[16,8,2176]{2,1,0:T(8,128)(2,1)S(1)}, u32[]{:S(2)}, u32[]{:S(2)}) %all-to-all-start) | async-done | bytes 557088 | tf_op jit(solution)/shard_map/all_to_all | solution.py:116
  35.4 0.3 fusion.29
  35.7 0.2 fusion.16
  35.9 1.6 %fusion.25 = f32[128,256]{1,0:T(8,128)S(1)} fusion(bf16[1,2048,256]{2,1,0:T(8,128)(2,1)} %param.38, bf16[128,2176]{1,0:T(8,128)(2,1)S(1)} %bitcast.60), kind=kOutput, calls=%fused_computation.33 | convolution fusion | flops 134217728 | bytes 1703936 | tf_op jit(solution)/shard_map/dot_general | solution.py:39
  37.5 3.3 %fusion.8 = f32[128,2048]{1,0:T(8,128)} fusion(bf16[1,256,2048]{2,1,0:T(8,128)(2,1)} %param.40, bf16[1,2048,256]{2,1,0:T(8,128)(2,1)} %param.39, bf16[128,2176]{1,0:T(8,128)(2,1)S(1)} %bitcast.61, f32[128,256]{1,0:T(8,128)S(1)} %fusion.25), kind=kOutput, calls=%fused_computation.13 | convolution fusion | flops 268632064 | bytes 3801088 | tf_op jit(solution)/shard_map/dot_general | solution.py:42
  40.8 1.5 %fusion.18 = f32[128,256]{1,0:T(8,128)S(1)} fusion(bf16[1,2048,256]{2,1,0:T(8,128)(2,1)} %collective-permute-done.1, bf16[128,2176]{1,0:T(8,128)(2,1)S(1)} %bitcast.62), kind=kOutput, calls=%fused_computation.27 | convolution fusion | flops 134217728 | bytes 1703936 | tf_op jit(solution)/shard_map/dot_general | solution.py:40
  42.4 3.7 %fusion.1 = f32[128,2048]{1,0:T(8,128)} fusion(f32[128,2048]{1,0:T(8,128)} %fusion.8, bf16[1,256,2048]{2,1,0:T(8,128)(2,1)} %collective-permute-done.2, f32[128]{0:T(128)S(1)} %convert_reduce_fusion.1, f32[128,256]{1,0:T(8,128)S(1)} %fusion.18, bf16[1,2048,256]{2,1,0:T(8,128)(2,1)} %collective-permute-done, bf16[128,2176]{1,0:T(8,128)(2,1)S(1)} %bitcast.63), kind=kOutput, calls=%fused_computation.3 | convolution fusion | flops 269156352 | bytes 4850176 | tf_op jit(solution)/shard_map/dot_general | solution.py:42
  46.1 2.7 %fusion.3 = bf16[16,8,2048]{2,1,0:T(8,128)(2,1)} fusion(f32[128,2048]{1,0:T(8,128)} %fusion.1, bf16[128,2048]{1,0:T(8,128)(2,1)S(1)} %copy-done.3, bf16[2048,128]{1,0:T(8,128)(2,1)} %param.34, f32[128]{0:T(128)S(1)} %fusion.16, bf16[128,2176]{1,0:T(8,128)(2,1)S(1)} %bitcast.64, f32[128,128]{1,0:T(8,128)S(1)} %fusion.29), kind=kOutput, calls=%fused_computation.5 | convolution fusion | flops 135102464 | bytes 3211776 | tf_op jit(solution)/shard_map/dot_general | solution.py:42
  48.8 4.1 %all-to-all-start.1 = ((bf16[16,8,2048]{2,1,0:T(8,128)(2,1)}), bf16[16,8,2048]{2,1,0:T(8,128)(2,1)S(1)}, u32[]{:S(2)}, u32[]{:S(2)}) async-start(bf16[16,8,2048]{2,1,0:T(8,128)(2,1)} %fusion.3), calls=%async_computation.1 | async-start | bytes 1048576 | tf_op jit(solution)/shard_map/all_to_all | solution.py:126
  52.9 14.4 %all-to-all-done.1 = bf16[16,8,2048]{2,1,0:T(8,128)(2,1)S(1)} async-done(((bf16[16,8,2048]{2,1,0:T(8,128)(2,1)}), bf16[16,8,2048]{2,1,0:T(8,128)(2,1)S(1)}, u32[]{:S(2)}, u32[]{:S(2)}) %all-to-all-start.1) | async-done | bytes 524320 | tf_op jit(solution)/shard_map/all_to_all | solution.py:126
  67.8 0.7 %multiply_convert_fusion.2 = bf16[8,2048]{1,0:T(8,128)(2,1)} fusion(f32[2048]{0:T(1024)S(1)} %convert_element_type.102, f32[8]{0:T(128)S(1)} %add_rsqrt_fusion, f32[8]{0:T(128)S(1)} %broadcast_multiply_fusion, f32[8,2048]{1,0:T(8,128)S(1)} %convert_reduce_fusion, f32[2048]{0:T(1024)S(1)} %convert_element_type.92, f32[8]{0:T(128)S(1)} %add_rsqrt_fusion.1, ...), kind=kLoop, calls=%fused_computation.52 | loop fusion | flops 180224 | bytes 180352 | tf_op jit(solution)/shard_map/convert_element_type | solution.py:134
  (66 shorter events, 2.8 us)
Async XLA Ops:
  0.0 3.7 %copy-start = (bf16[8,256,512]{2,1,0:T(8,128)(2,1)S(1)}, bf16[8,256,512]{2,1,0:T(8,128)(2,1)}, u32[]{:S(2)}) copy-start(bf16[8,256,512]{2,1,0:T(8,128)(2,1)} %param.26) | copy-start | bytes 6291460
  0.0 5.2 %copy-start.8 = (bf16[8,512]{1,0:T(8,128)(2,1)S(1)}, bf16[8,512]{1,0:T(8,128)(2,1)}, u32[]{:S(2)}) copy-start(bf16[8,512]{1,0:T(8,128)(2,1)} %param.24) | copy-start | bytes 24580
  0.0 5.2 %copy-start.5 = (bf16[8,8,512]{2,1,0:T(8,128)(2,1)S(1)}, bf16[8,8,512]{2,1,0:T(8,128)(2,1)}, u32[]{:S(2)}) copy-start(bf16[8,8,512]{2,1,0:T(8,128)(2,1)} %param.22) | copy-start | bytes 196612
  0.0 5.9 %copy-start.4 = (bf16[8,256,32]{1,2,0:T(8,128)(2,1)S(1)}, bf16[8,256,32]{1,2,0:T(8,128)(2,1)}, u32[]{:S(2)}) copy-start(bf16[8,256,32]{1,2,0:T(8,128)(2,1)} %param.27) | copy-start | bytes 393220
  3.7 3.1 %copy-start.1 = (bf16[512,8,64]{0,2,1:T(8,128)(2,1)S(1)}, bf16[512,8,64]{0,2,1:T(8,128)(2,1)}, u32[]{:S(2)}) copy-start(bf16[512,8,64]{0,2,1:T(8,128)(2,1)} %param.29) | copy-start | bytes 1572868
  5.2 2.0 %copy-start.6 = (bf16[8,2048]{1,0:T(8,128)(2,1)S(1)}, bf16[8,2048]{1,0:T(8,128)(2,1)}, u32[]{:S(2)}) copy-start(bf16[8,2048]{1,0:T(8,128)(2,1)} %param.21) | copy-start | bytes 98308
  6.3 3.2 %copy-start.9 = (bf16[2048]{0:T(1024)(128)(2,1)S(1)}, bf16[2048]{0:T(1024)(128)(2,1)}, u32[]{:S(2)}) copy-start(bf16[2048]{0:T(1024)(128)(2,1)} %param.31) | copy-start | bytes 12292
  6.4 3.2 %copy-start.7 = (f32[8,6]{1,0:T(8,128)S(1)}, f32[8,6]{1,0:T(8,128)}, u32[]{:S(2)}) copy-start(f32[8,6]{1,0:T(8,128)} %param.37) | copy-start | bytes 580
  6.4 3.4 %copy-start.12 = (s32[8,6]{1,0:T(8,128)S(1)}, s32[8,6]{1,0:T(8,128)}, u32[]{:S(2)}) copy-start(s32[8,6]{1,0:T(8,128)} %param.36) | copy-start | bytes 580
  7.2 13.1 %copy-start.10 = (bf16[2048]{0:T(1024)(128)(2,1)S(1)}, bf16[2048]{0:T(1024)(128)(2,1)}, u32[]{:S(2)}) copy-start(bf16[2048]{0:T(1024)(128)(2,1)} %param.32) | copy-start | bytes 12292
  9.3 26.1 %copy-start.2 = (bf16[2048,128]{1,0:T(8,128)(2,1)S(1)}, bf16[2048,128]{1,0:T(8,128)(2,1)}, u32[]{:S(2)}) copy-start(bf16[2048,128]{1,0:T(8,128)(2,1)} %param.33) | copy-start | bytes 1572868
  11.3 24.0 %all-to-all-start = ((bf16[16,8,2176]{2,1,0:T(8,128)(2,1)}), bf16[16,8,2176]{2,1,0:T(8,128)(2,1)S(1)}, u32[]{:S(2)}, u32[]{:S(2)}) async-start(bf16[16,8,2176]{2,1,0:T(8,128)(2,1)} %pad_maximum_fusion), calls=%async_computation | async-start | bytes 1114112 | tf_op jit(solution)/shard_map/all_to_all | solution.py:116
  19.6 21.2 %collective-permute-start.1 = (bf16[1,2048,256]{2,1,0:T(8,128)(2,1)}, bf16[1,2048,256]{2,1,0:T(8,128)(2,1)}, u32[]{:S(2)}, u32[]{:S(2)}) collective-permute-start(bf16[1,2048,256]{2,1,0:T(8,128)(2,1)} %param.39), channel_id=1, source_target_pairs={{0,1},{1,0},{2,3},{3,2},{4,5},{5,4},{6,7},{7,6},{8,9},{9,8},{10,11... | collective-permute-start | bytes 3145736 | tf_op jit(solution)/shard_map/ppermute | solution.py:73
  19.7 22.6 %collective-permute-start = (bf16[1,2048,256]{2,1,0:T(8,128)(2,1)}, bf16[1,2048,256]{2,1,0:T(8,128)(2,1)}, u32[]{:S(2)}, u32[]{:S(2)}) collective-permute-start(bf16[1,2048,256]{2,1,0:T(8,128)(2,1)} %param.38), channel_id=1, source_target_pairs={{0,1},{1,0},{2,3},{3,2},{4,5},{5,4},{6,7},{7,6},{8,9},{9,8},{10,11... | collective-permute-start | bytes 3145736 | tf_op jit(solution)/shard_map/ppermute | solution.py:72
  20.2 22.2 %collective-permute-start.2 = (bf16[1,256,2048]{2,1,0:T(8,128)(2,1)}, bf16[1,256,2048]{2,1,0:T(8,128)(2,1)}, u32[]{:S(2)}, u32[]{:S(2)}) collective-permute-start(bf16[1,256,2048]{2,1,0:T(8,128)(2,1)} %param.40), channel_id=1, source_target_pairs={{0,1},{1,0},{2,3},{3,2},{4,5},{5,4},{6,7},{7,6},{8,9},{9,8},{10,11... | collective-permute-start | bytes 3145736 | tf_op jit(solution)/shard_map/ppermute | solution.py:74
  42.3 3.7 %copy-start.3 = (bf16[128,2048]{1,0:T(8,128)(2,1)S(1)}, bf16[128,2048]{1,0:T(8,128)(2,1)}, u32[]{:S(2)}) copy-start(bf16[128,2048]{1,0:T(8,128)(2,1)} %param.35) | copy-start | bytes 1572868
  46.0 6.8 %copy-start.11 = (bf16[2048]{0:T(1024)(128)(2,1)S(1)}, bf16[2048]{0:T(1024)(128)(2,1)}, u32[]{:S(2)}) copy-start(bf16[2048]{0:T(1024)(128)(2,1)} %param.41) | copy-start | bytes 12292
  48.8 18.5 %all-to-all-start.1 = ((bf16[16,8,2048]{2,1,0:T(8,128)(2,1)}), bf16[16,8,2048]{2,1,0:T(8,128)(2,1)S(1)}, u32[]{:S(2)}, u32[]{:S(2)}) async-start(bf16[16,8,2048]{2,1,0:T(8,128)(2,1)} %fusion.3), calls=%async_computation.1 | async-start | bytes 1048576 | tf_op jit(solution)/shard_map/all_to_all | solution.py:126

commit v2 on v1

--- a/solution.py
+++ b/solution.py
@@ -1,6 +1,8 @@
 import jax
 import jax.numpy as jnp
 from jax import lax
+from jax.experimental import pallas as pl
+from jax.experimental.pallas import tpu as pltpu
 from jax.sharding import PartitionSpec as P
 
 NOPE = 64
@@ -35,11 +37,64 @@
     return (values - center) * lax.rsqrt(spread + EPS) * gain.astype(jnp.float32)
 
 
-def gated(rows, gate_weight, up_weight, down_weight):
-    gate_pre = jnp.dot(rows, gate_weight, preferred_element_type=jnp.float32)
-    up_pre = jnp.dot(rows, up_weight, preferred_element_type=jnp.float32)
-    hidden = (jax.nn.silu(gate_pre) * up_pre).astype(jnp.bfloat16)
-    return jnp.dot(hidden, down_weight, preferred_element_type=jnp.float32)
+def branch_kernel(arrived, mix_gate, *refs):
+    weights, out, held, total, sems = refs[:9], refs[9], refs[10:19], refs[19], refs[20]
+    row_count, model_width = out.shape
+    copies = [
+        pltpu.make_async_copy(weights[i], held[i], sems.at[i]) for i in range(len(weights))
+    ]
+    for copy in copies:
+        copy.start()
+    block = min(row_count, 128)
+
+    def stage(number):
+        for copy in copies[3 * number : 3 * number + 3]:
+            copy.wait()
+        gate_weight, up_weight, down_weight = held[3 * number : 3 * number + 3]
+
+        def piece(index, carry):
+            place = pl.ds(pl.multiple_of(index * block, block), block)
+            rows = arrived[place, :model_width]
+            gate_pre = jnp.dot(rows, gate_weight[...], preferred_element_type=jnp.float32)
+            up_pre = jnp.dot(rows, up_weight[...], preferred_element_type=jnp.float32)
+            hidden = (jax.nn.silu(gate_pre) * up_pre).astype(jnp.bfloat16)
+            part = jnp.dot(hidden, down_weight[...], preferred_element_type=jnp.float32)
+            if number == 0:
+                pre = rows.astype(jnp.float32) * mix_gate[...].astype(jnp.float32)
+                total[place, :] = part * jax.nn.sigmoid(jnp.sum(pre, -1, keepdims=True))
+            else:
+                tail = arrived[place, model_width:].astype(jnp.float32)
+                value = total[place, :] + part * jnp.sum(tail, -1, keepdims=True)
+                if number == 1:
+                    total[place, :] = value
+                else:
+                    out[place, :] = value.astype(jnp.bfloat16)
+            return carry
+
+        if row_count == block:
+            piece(0, 0)
+        else:
+            lax.fori_loop(0, row_count // block, piece, 0)
+
+    for number in range(3):
+        stage(number)
+
+
+def branches(arrived, mix_gate, weights, model_width):
+    row_count = arrived.shape[0]
+    return pl.pallas_call(
+        branch_kernel,
+        out_shape=jax.ShapeDtypeStruct((row_count, model_width), jnp.bfloat16),
+        in_specs=[pl.BlockSpec(memory_space=pltpu.VMEM)] * 2
+        + [pl.BlockSpec(memory_space=pl.ANY)] * len(weights),
+        out_specs=pl.BlockSpec(memory_space=pltpu.VMEM),
+        scratch_shapes=[pltpu.VMEM(weight.shape, weight.dtype) for weight in weights]
+        + [
+            pltpu.VMEM((row_count, model_width), jnp.float32),
+            pltpu.SemaphoreType.DMA((len(weights),)),
+        ],
+        compiler_params=pltpu.CompilerParams(vmem_limit_bytes=56 << 20),
+    )(arrived, mix_gate, *weights)
 
 
 def on_device(
@@ -115,14 +170,22 @@
     )
     arrived = lax.all_to_all(outgoing, "ep", split_axis=0, concat_axis=0, tiled=True)
     arrived = arrived.reshape(ep_count * seq_count, model_width + LANES)
-    rows = arrived[:, :model_width]
-    weight = jnp.sum(arrived[:, model_width:].astype(jnp.float32), -1, keepdims=True)
-    partial_value = gated(rows, expert_gate[0], expert_up[0], expert_down[0]) + gated(
-        rows, other_gate[0], other_up[0], other_down[0]
-    )
-    mix = jax.nn.sigmoid(jnp.dot(rows, mix_gate, preferred_element_type=jnp.float32))
-    dense_part = gated(rows, dense_w_gate, dense_w_up, dense_w_down)
-    combined = (weight * partial_value + mix[:, None] * dense_part).astype(jnp.bfloat16)
+    combined = branches(
+        arrived,
+        mix_gate[None],
+        (
+            dense_w_gate,
+            dense_w_up,
+            dense_w_down,
+            expert_gate[0],
+            expert_up[0],
+            expert_down[0],
+            other_gate[0],
+            other_up[0],
+            other_down[0],
+        ),
+        model_width,
+    )
     returned = lax.all_to_all(
         combined.reshape(ep_count, seq_count, model_width),
         "ep",

time: 69.1 us -> 63.3 us (0.916)
  matrix products: 18.2 us -> 4.91 us
  Pallas kernels: 0 us -> 5.91 us
  local copies, waits for them, and re-layouts: 0.57 us -> 1.93 us
    dot_general x7 -> x0, matrix products: 13.3 us -> none  [the longest x3 9.72 us: gated(): return jnp.dot(hidden, down_weight, preferred_element_type=jnp.float32)]
    pallas_call x0 -> x1, Pallas kernels: none -> 5.91 us  [branches(): pl.pallas_call(branch_kernel, out_shape=jax.ShapeDtypeStruct((row_count,...]
    unnamed x28 -> x25, local copies, waits for them, and re-layouts: 0.16 us -> 0.92 us
  transfers between devices with their start and end apart: 5 -> 5, of which waited for: 2 -> 2; matrix products, arithmetic and copies ran while one was open for 10% -> 18% of each run, Pallas kernels for 0% -> 0%
where the time goes in v2:
time: 63.3 us; the launch traced here: 62.8 us
  waiting for transfers between devices  29.8 us (47%)
  starting transfers between devices  13.3 us (21%)
  other arithmetic  6.71 us (11%)
  Pallas kernels  5.91 us (9%)
  matrix products  4.91 us (8%)
  local copies, waits for them, and re-layouts  1.93 us (3%)
    all_to_all x1, waiting for transfers between devices, on_device(): lax.all_to_all(outgoing, 'ep', split_axis=0, concat_axis=0, tiled=True)  15.5 us
    all_to_all x1, waiting for transfers between devices, on_device(): lax.all_to_all(combined.reshape(ep_count, seq_count, model_width), 'ep',...  14.4 us
    all_to_all x1, starting transfers between devices, on_device(): lax.all_to_all(outgoing, 'ep', split_axis=0, concat_axis=0, tiled=True)  7.96 us
    pallas_call x1, Pallas kernels, branches(): pl.pallas_call(branch_kernel, out_shape=jax.ShapeDtypeStruct((row_count,...  5.91 us
    all_to_all x1, starting transfers between devices, on_device(): lax.all_to_all(combined.reshape(ep_count, seq_count, model_width), 'ep',...  4.24 us
    dot_general x1, matrix products, on_device(): jnp.dot(heads_out, out_proj, preferred_element_type=jnp.float32)  2.1 us
    dot_general x1, matrix products, on_device(): jnp.einsum('bhr,btr->bht', query_latent, latent_cache, preferred_element_...  1.53 us
  transfers between devices with their start and end apart: 5, of which 2 were waited for; matrix products, arithmetic and copies ran while one was open for 18% of the time, Pallas kernels for 0%

profile of v2, /device:TPU:0, one launch (start us, length us, event | category | flops | bytes accessed | tf_op | source)
XLA Modules:
  0.0 62.8 jit_solution(9175214162354372840)
XLA Ops:
  0.0 0.6 collective-permute-start
  0.7 0.4 collective-permute-start.2
  1.1 0.7 %convert_element_type.66 = f32[8]{0:T(128)S(1)} convert(s32[8]{0:T(128)} %param.28) | non-fusion elementwise | flops 8 | bytes 64 | tf_op jit(solution)/shard_map/convert_element_type | solution.py:20
  1.8 0.7 %iota_compare_fusion.1 = pred[8,256]{1,0:T(8,128)(4,1)S(1)} fusion(s32[8]{0:T(128)} %param.28), kind=kLoop, calls=%fused_computation.32 | loop fusion | flops 2048 | bytes 2080 | tf_op jit(solution)/shard_map/lt | solution.py:141
  2.5 0.7 %convert_element_type.67 = f32[8,32]{1,0:T(8,128)S(1)} convert(bf16[8,32]{1,0:T(8,128)(2,1)} %param.25) | non-fusion elementwise | flops 256 | bytes 1536 | tf_op jit(solution)/shard_map/convert_element_type | solution.py:132
  3.2 0.7 %convert_element_type.65 = f32[8,8,32]{2,1,0:T(8,128)S(1)} convert(bf16[8,8,32]{2,1,0:T(8,128)(2,1)} %param.23) | non-fusion elementwise | flops 2048 | bytes 12288 | tf_op jit(solution)/shard_map/convert_element_type | solution.py:131
  3.9 0.7 %convert_element_type.71 = f32[8,512]{1,0:T(8,128)S(1)} convert(bf16[8,512]{1,0:T(8,128)(2,1)} %param.24) | non-fusion elementwise | flops 4096 | bytes 24576 | tf_op jit(solution)/shard_map/convert_element_type | solution.py:151
  4.6 1.5 %fusion.23 = f32[8,8,256]{2,1,0:T(8,128)S(1)} fusion(bf16[8,8,512]{2,1,0:T(8,128)(2,1)} %param.22, bf16[8,256,512]{2,1,0:T(8,128)(2,1)S(1)} %copy-done), kind=kOutput, calls=%fused_computation.60 | convolution fusion | flops 16777216 | bytes 2228224 | tf_op jit(solution)/shard_map/bhr,btr->bht/dot_general | solution.py:134
  6.8 0.3 fusion.21
  7.3 0.4 fusion.2
  7.7 0.2 fusion.5
  8.1 2.1 %fusion.22 = (f32[8]{0:T(128)S(1)}, f32[8,2048]{1,0:T(8,128)S(1)}) fusion(bf16[8,512]{1,0:T(8,128)(2,1)S(1)} %reshape.135, bf16[512,2048]{1,0:T(8,128)(2,1)} %param.30, bf16[8,2048]{1,0:T(8,128)(2,1)S(1)} %copy-done.5), kind=kOutput, calls=%fused_computation.59 | convolution fusion | flops 16875512 | bytes 2203680 | tf_op jit(solution)/shard_map/dot_general | solution.py:155
  10.2 0.2 multiply_reduce_fusion.1
  11.3 0.8 %pad_maximum_fusion = bf16[16,8,2176]{2,1,0:T(8,128)(2,1)} fusion(bf16[16,8,128]{2,1,0:T(8,128)(2,1)S(1)} %select_convert_fusion, bf16[16,8,2048]{2,1,0:T(8,128)(2,1)S(1)} %broadcast_in_dim.47), kind=kLoop, calls=%fused_computation.11 | loop fusion | flops 1114112 | bytes 1114112 | tf_op jit(solution)/shard_map/concatenate | solution.py:168
  12.2 8.0 %all-to-all-start = ((bf16[16,8,2176]{2,1,0:T(8,128)(2,1)}), bf16[16,8,2176]{2,1,0:T(8,128)(2,1)S(1)}, u32[]{:S(2)}, u32[]{:S(2)}) async-start(bf16[16,8,2176]{2,1,0:T(8,128)(2,1)} %pad_maximum_fusion), calls=%async_computation | async-start | bytes 1114112 | tf_op jit(solution)/shard_map/all_to_all | solution.py:171
  20.2 0.6 broadcast_in_dim.56.mix_gate
  20.8 15.5 %all-to-all-done = bf16[16,8,2176]{2,1,0:T(8,128)(2,1)S(1)} async-done(((bf16[16,8,2176]{2,1,0:T(8,128)(2,1)}), bf16[16,8,2176]{2,1,0:T(8,128)(2,1)S(1)}, u32[]{:S(2)}, u32[]{:S(2)}) %all-to-all-start) | async-done | bytes 557088 | tf_op jit(solution)/shard_map/all_to_all | solution.py:171
  36.2 0.8 %copy-done.1 = bf16[16,8,2176]{2,1,0:T(8,128)(2,1)} copy-done((bf16[16,8,2176]{2,1,0:T(8,128)(2,1)}, bf16[16,8,2176]{2,1,0:T(8,128)(2,1)S(1)}, u32[]{:S(2)}) %copy-start.1) | copy-done | bytes 557080
  37.0 5.9 %shard_map.199 = bf16[128,2048]{1,0:T(8,128)(2,1)} custom-call(bf16[128,2176]{1,0:T(8,128)(2,1)} %bitcast.25, bf16[1,2048]{1,0:T(2,128)(2,1)} %broadcast_in_dim.56.mix_gate, bf16[2048,128]{1,0:T(8,128)(2,1)} %refs_0_.1, bf16[2048,128]{1,0:T(8,128)(2,1)} %refs_1_.1, bf16[128,2048]{1,0:T(8,128)(2,1)} %refs_2_.1, bf16[2048,256]{1,0:T(8,128)(2,1)} %bitcast.27, ...), custom_call_target="tpu_custom_call" | custom-call | tf_op jit(solution)/shard_map/pallas_call | solution.py:85
  42.9 4.2 %all-to-all-start.1 = ((bf16[16,8,2048]{2,1,0:T(8,128)(2,1)}), bf16[16,8,2048]{2,1,0:T(8,128)(2,1)S(1)}, u32[]{:S(2)}, u32[]{:S(2)}) async-start(bf16[16,8,2048]{2,1,0:T(8,128)(2,1)} %bitcast.26), calls=%async_computation.1 | async-start | bytes 1048576 | tf_op jit(solution)/shard_map/all_to_all | solution.py:189
  47.2 14.4 %all-to-all-done.1 = bf16[16,8,2048]{2,1,0:T(8,128)(2,1)S(1)} async-done(((bf16[16,8,2048]{2,1,0:T(8,128)(2,1)}), bf16[16,8,2048]{2,1,0:T(8,128)(2,1)S(1)}, u32[]{:S(2)}, u32[]{:S(2)}) %all-to-all-start.1) | async-done | bytes 524320 | tf_op jit(solution)/shard_map/all_to_all | solution.py:189
  61.7 0.2 fusion.10
  61.9 0.2 multiply_reduce_fusion
  62.1 0.7 %multiply_convert_fusion = bf16[8,2048]{1,0:T(8,128)(2,1)} fusion(f32[2048]{0:T(1024)S(1)} %convert_element_type.82, f32[8]{0:T(128)S(1)} %add_rsqrt_fusion, f32[8]{0:T(128)S(1)} %broadcast_multiply_fusion, f32[8,2048]{1,0:T(8,128)S(1)} %convert_reduce_fusion, f32[2048]{0:T(1024)S(1)} %convert_element_type.77, f32[8]{0:T(128)S(1)} %add_rsqrt_fusion.1, ...), kind=kLoop, calls=%fused_computation.13 | loop fusion | flops 180224 | bytes 180352 | tf_op jit(solution)/shard_map/convert_element_type | solution.py:197
  (57 shorter events, 2.0 us)
Async XLA Ops:
  0.0 4.6 %copy-start = (bf16[8,256,512]{2,1,0:T(8,128)(2,1)S(1)}, bf16[8,256,512]{2,1,0:T(8,128)(2,1)}, u32[]{:S(2)}) copy-start(bf16[8,256,512]{2,1,0:T(8,128)(2,1)} %param.26) | copy-start | bytes 6291460
  0.0 6.1 %copy-start.7 = (bf16[8,512]{1,0:T(8,128)(2,1)S(1)}, bf16[8,512]{1,0:T(8,128)(2,1)}, u32[]{:S(2)}) copy-start(bf16[8,512]{1,0:T(8,128)(2,1)} %param.24) | copy-start | bytes 24580
  0.0 6.2 %copy-start.4 = (bf16[8,8,512]{2,1,0:T(8,128)(2,1)S(1)}, bf16[8,8,512]{2,1,0:T(8,128)(2,1)}, u32[]{:S(2)}) copy-start(bf16[8,8,512]{2,1,0:T(8,128)(2,1)} %param.22) | copy-start | bytes 196612
  0.0 6.8 %copy-start.3 = (bf16[8,256,32]{1,2,0:T(8,128)(2,1)S(1)}, bf16[8,256,32]{1,2,0:T(8,128)(2,1)}, u32[]{:S(2)}) copy-start(bf16[8,256,32]{1,2,0:T(8,128)(2,1)} %param.27) | copy-start | bytes 393220
  0.0 36.2 %collective-permute-start = (bf16[1,2048,256]{2,1,0:T(8,128)(2,1)}, bf16[1,2048,256]{2,1,0:T(8,128)(2,1)}, u32[]{:S(2)}, u32[]{:S(2)}) collective-permute-start(bf16[1,2048,256]{2,1,0:T(8,128)(2,1)} %param.38), channel_id=1, source_target_pairs={{0,1},{1,0},{2,3},{3,2},{4,5},{5,4},{6,7},{7,6},{8,9},{9,8},{10,11... | collective-permute-start | bytes 3145736 | tf_op jit(solution)/shard_map/ppermute | solution.py:127
  0.6 35.6 %collective-permute-start.1 = (bf16[1,2048,256]{2,1,0:T(8,128)(2,1)}, bf16[1,2048,256]{2,1,0:T(8,128)(2,1)}, u32[]{:S(2)}, u32[]{:S(2)}) collective-permute-start(bf16[1,2048,256]{2,1,0:T(8,128)(2,1)} %param.39), channel_id=1, source_target_pairs={{0,1},{1,0},{2,3},{3,2},{4,5},{5,4},{6,7},{7,6},{8,9},{9,8},{10,11... | collective-permute-start | bytes 3145736 | tf_op jit(solution)/shard_map/ppermute | solution.py:128
  0.7 35.6 %collective-permute-start.2 = (bf16[1,256,2048]{2,1,0:T(8,128)(2,1)}, bf16[1,256,2048]{2,1,0:T(8,128)(2,1)}, u32[]{:S(2)}, u32[]{:S(2)}) collective-permute-start(bf16[1,256,2048]{2,1,0:T(8,128)(2,1)} %param.40), channel_id=1, source_target_pairs={{0,1},{1,0},{2,3},{3,2},{4,5},{5,4},{6,7},{7,6},{8,9},{9,8},{10,11... | collective-permute-start | bytes 3145736 | tf_op jit(solution)/shard_map/ppermute | solution.py:129
  4.6 3.1 %copy-start.2 = (bf16[512,8,64]{0,2,1:T(8,128)(2,1)S(1)}, bf16[512,8,64]{0,2,1:T(8,128)(2,1)}, u32[]{:S(2)}) copy-start(bf16[512,8,64]{0,2,1:T(8,128)(2,1)} %param.29) | copy-start | bytes 1572868
  6.1 2.0 %copy-start.5 = (bf16[8,2048]{1,0:T(8,128)(2,1)S(1)}, bf16[8,2048]{1,0:T(8,128)(2,1)}, u32[]{:S(2)}) copy-start(bf16[8,2048]{1,0:T(8,128)(2,1)} %param.21) | copy-start | bytes 98308
  7.3 3.2 %copy-start.8 = (bf16[2048]{0:T(1024)(128)(2,1)S(1)}, bf16[2048]{0:T(1024)(128)(2,1)}, u32[]{:S(2)}) copy-start(bf16[2048]{0:T(1024)(128)(2,1)} %param.31) | copy-start | bytes 12292
  7.3 3.2 %copy-start.6 = (f32[8,6]{1,0:T(8,128)S(1)}, f32[8,6]{1,0:T(8,128)}, u32[]{:S(2)}) copy-start(f32[8,6]{1,0:T(8,128)} %param.37) | copy-start | bytes 580
  7.3 3.4 %copy-start.11 = (s32[8,6]{1,0:T(8,128)S(1)}, s32[8,6]{1,0:T(8,128)}, u32[]{:S(2)}) copy-start(s32[8,6]{1,0:T(8,128)} %param.36) | copy-start | bytes 580
  8.1 12.1 %copy-start.9 = (bf16[2048]{0:T(1024)(128)(2,1)S(1)}, bf16[2048]{0:T(1024)(128)(2,1)}, u32[]{:S(2)}) copy-start(bf16[2048]{0:T(1024)(128)(2,1)} %param.32) | copy-start | bytes 12292
  12.2 24.0 %all-to-all-start = ((bf16[16,8,2176]{2,1,0:T(8,128)(2,1)}), bf16[16,8,2176]{2,1,0:T(8,128)(2,1)S(1)}, u32[]{:S(2)}, u32[]{:S(2)}) async-start(bf16[16,8,2176]{2,1,0:T(8,128)(2,1)} %pad_maximum_fusion), calls=%async_computation | async-start | bytes 1114112 | tf_op jit(solution)/shard_map/all_to_all | solution.py:171
  36.2 0.8 %copy-start.1 = (bf16[16,8,2176]{2,1,0:T(8,128)(2,1)}, bf16[16,8,2176]{2,1,0:T(8,128)(2,1)S(1)}, u32[]{:S(2)}) copy-start(bf16[16,8,2176]{2,1,0:T(8,128)(2,1)S(1)} %all-to-all-done) | copy-start | bytes 1671172
  37.0 10.2 %copy-start.10 = (bf16[2048]{0:T(1024)(128)(2,1)S(1)}, bf16[2048]{0:T(1024)(128)(2,1)}, u32[]{:S(2)}) copy-start(bf16[2048]{0:T(1024)(128)(2,1)} %param.41) | copy-start | bytes 12292
  42.9 18.6 %all-to-all-start.1 = ((bf16[16,8,2048]{2,1,0:T(8,128)(2,1)}), bf16[16,8,2048]{2,1,0:T(8,128)(2,1)S(1)}, u32[]{:S(2)}, u32[]{:S(2)}) async-start(bf16[16,8,2048]{2,1,0:T(8,128)(2,1)} %bitcast.26), calls=%async_computation.1 | async-start | bytes 1048576 | tf_op jit(solution)/shard_map/all_to_all | solution.py:189
